TPU v7x, 512 devices: a whole 4x8x8 slice. The times are simulated.
512 devices in a mesh: sp: 128 (over z, y, core), tp: 4 (over x).
Axes of the slice: x: 4, y: 8, z: 8, core: 2. Of those that a mesh axis runs over, the one named last changes fastest.
Arguments:
- tokens: bfloat16 [65536, 2048], P(('sp', 'tp')), may hold values from -6 to 6
- pooling_input_weight: bfloat16 [2048, 1024], P('sp', 'tp'), may hold values from -0.125 to 0.125
- query_matrix: bfloat16 [2048, 512], P('sp', 'tp'), may hold values from -0.125 to 0.125
- key_matrix: bfloat16 [2048, 512], P('sp', 'tp'), may hold values from -0.125 to 0.125
- value_matrix: bfloat16 [2048, 1024], P('sp', 'tp'), may hold values from -0.125 to 0.125
- decay_inner_weight: bfloat16 [2048, 64], replicated, may hold values from -0.125 to 0.125
- decay_outer_weight: bfloat16 [2, 32, 512], replicated, may hold values from -1 to 1
- channel_decay_bias: float32 [2, 512], replicated, may hold values from -0.3 to 12
- spike_log_decay: float32 [8, 65536], P('tp', 'sp'), may hold values from -0.72 to 0
- starting_state: float32 [2, 8, 64, 128], P(None, 'tp'), may hold values from -1536 to 1536
- pooling_group_map: bfloat16 [4, 256, 256], replicated, may hold values from -0.375 to 0.375
- pooling_output_weight: bfloat16 [1024, 2048], P('tp', 'sp'), may hold values from -0.125 to 0.125
- attention_output_weight: bfloat16 [1024, 2048], P('tp', 'sp'), may hold values from -0.125 to 0.125
Outputs:
- mixed: bfloat16 [65536, 2048], P(('sp', 'tp'))
All inputs are finite; a program needn't handle non-finite values.
Results may differ from a plain program's by a relative error of at most 0.015.
Values may be sent and summed in bfloat16 or wider, within the bound.
No kernel may reach another device: no remote copies, remote signals or barrier semaphores. Data moves between devices by JAX's collectives and lax.ppermute only.
A program may use at most 64 MiB of HBM per device.

v0:
```python
import jax
import jax.numpy as jnp
from jax import lax
from jax.sharding import Mesh
from jax.sharding import PartitionSpec as P

KEY_CHANNELS = 64
DV = 128
RANK = 32
BLOCK = 64
SP = ("sp_0", "sp_1", "sp_2")
SP_TP = ("sp_0", "sp_1", "sp_2", "tp")
eps_value = 1e-06
gate_norm_factor = 16.0
rim_width = 8


def from_everyone(value, axis):
    copies = jnp.broadcast_to(value, (lax.axis_size(axis), *value.shape))
    return lax.all_to_all(copies, axis, split_axis=0, concat_axis=0, tiled=True)


def laid_out(tiles, dim):
    tiles = jnp.moveaxis(tiles, 0, dim)
    lengths = tiles.shape
    return tiles.reshape(*lengths[:dim], lengths[dim] * lengths[dim + 1], *lengths[dim + 2 :])


def gathered_copies(value, axis, dim):
    tiles = from_everyone(value, axis)
    return laid_out(tiles, dim)


def extended(value, sides, width):
    for axis, dim in sides:
        devices, length = (lax.axis_size(axis), value.shape[dim])
        up = [(i, (i + 1) % devices) for i in range(devices - 1)]
        down = [(j, i) for i, j in up]
        last = lax.slice_in_dim(value, length - width, length, axis=dim)
        leading = lax.slice_in_dim(value, 0, width, axis=dim)
        before = lax.ppermute(last, axis, up)
        after = lax.ppermute(leading, axis, down)
        value = jnp.concatenate([before, value, after], axis=dim)
    return value


def neutral_like(value, identity):
    return jax.tree.map(
        lambda a, e: jnp.broadcast_to(jnp.asarray(e, a.dtype), a.shape), value, identity
    )


def carried_in(value, axes, combine, identity):
    before = start = neutral_like(value, identity)
    total = value
    for axis in reversed(axes):
        devices, mine = (lax.axis_size(axis), lax.axis_index(axis))
        pieces = jax.tree.map(
            lambda part, kind: lax.all_gather(part.astype(kind), axis),
            total,
            jax.tree.map(lambda a: jnp.bfloat16 if a.dtype == jnp.float32 else a.dtype, value),
        )
        inside, total = (start, start)
        for k in range(devices):
            passed = k < mine
            total = combine(
                total, jax.tree.map(lambda part, own: part[k].astype(own.dtype), pieces, value)
            )
            inside = jax.tree.map(lambda new, old: jnp.where(passed, new, old), total, inside)
        before = combine(inside, before)
    return before


def gathered_once(value, axis):
    leaves = jax.tree.leaves(value)
    order = sorted(range(len(leaves)), key=lambda k: -leaves[k].size)
    width = (1, *leaves[order[0]].shape)[-1]
    lines = [
        jnp.pad(leaves[k].reshape(-1), (0, -leaves[k].size % width)).reshape(-1, width)
        for k in order
    ]
    both, at, found = (lax.all_gather(jnp.concatenate(lines), axis), 0, {})
    for k, line in zip(order, lines):
        section = both[:, at : at + len(line)].reshape(len(both), -1)
        found[k] = section[:, : leaves[k].size].reshape(-1, *leaves[k].shape)
        at += len(line)
    numbers = iter(range(len(leaves)))
    return jax.tree.map(lambda _: found[next(numbers)], value)


def carried_in_2(value, axes, combine, identity):
    before = start = neutral_like(value, identity)
    total = value
    for axis in reversed(axes):
        devices, mine = (lax.axis_size(axis), lax.axis_index(axis))
        pieces = gathered_once(
            jax.tree.map(
                lambda part, kind: part.astype(kind),
                total,
                jax.tree.map(lambda a: jnp.bfloat16 if a.dtype == jnp.float32 else a.dtype, value),
            ),
            axis,
        )
        inside, total = (start, start)
        for k in reversed(range(devices)):
            passed = k > mine
            total = combine(
                total, jax.tree.map(lambda part, own: part[k].astype(own.dtype), pieces, value)
            )
            inside = jax.tree.map(lambda new, old: jnp.where(passed, new, old), total, inside)
        before = combine(inside, before)
    return before


def gather_turned(arrays, axis, dims):
    turned = [jnp.moveaxis(a, dim, 0) for a, dim in zip(arrays, dims)]
    both = jnp.concatenate([t.reshape(len(t), -1) for t in turned], axis=1)
    filled, at, finished = (lax.all_gather(both, axis, axis=0, tiled=True), 0, [])
    for t, dim in zip(turned, dims):
        section = filled[:, at : at + t[0].size].reshape(-1, *t.shape[1:])
        finished.append(jnp.moveaxis(section, 0, dim))
        at += t[0].size
    return tuple(finished)


def cut_along(value, dim, devices):
    lengths = value.shape
    tiles = value.reshape(*lengths[:dim], devices, lengths[dim] // devices, *lengths[dim + 1 :])
    return jnp.moveaxis(tiles, dim, 0)


def sum_at_owner(value, axis, dim):
    devices = lax.axis_size(axis)
    tiles = lax.all_to_all(cut_along(value, dim, devices), axis, 0, 0, tiled=True)
    return jnp.sum(tiles.astype(jnp.float32), axis=0)


def normalize(token_rows):
    floats = token_rows.astype(jnp.float32)
    scaled = floats * lax.rsqrt(jnp.mean(floats * floats, axis=-1, keepdims=True) + eps_value)
    return scaled.astype(jnp.bfloat16)


def chain_combine(earlier, later):
    return (earlier[0] + later[0], jnp.exp(later[0])[..., None] * earlier[1] + later[1])


def local_chain(decays, updates, backward):

    def advance(carried, element):
        log_total, memory = carried
        decay_now, update_now = element
        return (
            (log_total + decay_now, jnp.exp(decay_now)[..., None] * memory + update_now),
            (log_total, memory),
        )

    begin = (jnp.zeros_like(decays[0]), jnp.zeros_like(updates[0]))
    return lax.scan(advance, begin, (decays, updates), reverse=backward)


def within_blocks(queries, cumulative, key_rows, value_rows, lower):
    row_ids = lax.broadcasted_iota(jnp.int32, (BLOCK, BLOCK), 0)
    col_ids = lax.broadcasted_iota(jnp.int32, (BLOCK, BLOCK), 1)
    allowed = col_ids <= row_ids if lower else col_ids > row_ids
    scaled_q = queries * jnp.exp(cumulative)
    scaled_k = key_rows * jnp.exp(-cumulative)
    scores = jnp.einsum("hnid,hnjd->hnij", scaled_q, scaled_k)
    scores = jnp.where(allowed, scores, 0.0)
    return (scaled_q, jnp.einsum("hnij,hnjv->hniv", scores, value_rows))


def block_updates(key_rows, value_rows, cumulative, edge):
    weighted = key_rows * jnp.exp(edge[:, :, None, :] - cumulative)
    return jnp.einsum("hncd,hncv->hndv", weighted, value_rows)


def carried_term(scaled_q, before, entering):
    log_before, memory_before = before
    block_memory = jnp.exp(log_before)[..., None] * entering[None] + memory_before
    return jnp.einsum("hnid,nhdv->hniv", scaled_q, block_memory)


def shards(
    tokens,
    pooling_input_weight,
    query_matrix,
    key_matrix,
    value_matrix,
    decay_inner_weight,
    decay_outer_weight,
    channel_decay_bias,
    spike_log_decay,
    starting_state,
    pooling_group_map,
    pooling_output_weight,
    attention_output_weight,
):
    sp_index = lax.axis_index(SP)
    tp_index = lax.axis_index("tp")
    normed = normalize(tokens)
    pool_cols = pooling_input_weight.shape[1]
    qk_cols = query_matrix.shape[1]
    value_cols = value_matrix.shape[1]
    local_weight = jnp.concatenate(
        [pooling_input_weight, query_matrix, key_matrix, value_matrix], axis=1
    )
    all_rows = gathered_copies(normed, "tp", 0)
    summed = jnp.dot(
        all_rows,
        lax.all_gather(local_weight, SP, axis=0, tiled=True),
        preferred_element_type=jnp.float32,
    )
    rank_part = jnp.dot(all_rows, decay_inner_weight, preferred_element_type=jnp.float32).astype(
        jnp.bfloat16
    )
    projected = jnp.concatenate([summed.astype(jnp.bfloat16), rank_part], axis=1)
    sequence_length = projected.shape[0]
    blocks = sequence_length // BLOCK
    heads_here = qk_cols // KEY_CHANNELS
    pool_input = projected[:, :pool_cols]
    query_part = projected[:, pool_cols : pool_cols + qk_cols]
    key_part = projected[:, pool_cols + qk_cols : pool_cols + 2 * qk_cols]
    value_part = projected[:, pool_cols + 2 * qk_cols : pool_cols + 2 * qk_cols + value_cols]
    low_rank = projected[:, pool_cols + 2 * qk_cols + value_cols :]
    window = jnp.left_shift(jnp.int32(2), tp_index)
    half_width = window // 2
    padded = extended(pool_input, ((SP, 0),), rim_width)
    floats = padded.astype(jnp.float32)
    window_sum = jnp.zeros((sequence_length, pool_cols), jnp.float32)
    for offset in range(-rim_width, rim_width):
        inside = ((offset >= -half_width) & (offset < window - half_width)).astype(jnp.float32)
        window_sum = (
            window_sum + inside * floats[rim_width + offset : rim_width + offset + sequence_length]
        )
    seq_length = sequence_length * lax.axis_size(SP)
    position = sp_index * sequence_length + jnp.arange(sequence_length, dtype=jnp.int32)
    low_end = jnp.clip(position - half_width, 0, seq_length - 1)
    high_end = jnp.clip(position - half_width + window - 1, 0, seq_length - 1)
    counted = (high_end - low_end + 1).astype(jnp.float32)[:, None]
    pooled = (window_sum / counted - floats[rim_width : rim_width + sequence_length]).astype(
        jnp.bfloat16
    )
    mix_here = lax.dynamic_index_in_dim(pooling_group_map, tp_index, 0, keepdims=False)
    pool_output = jnp.dot(pooled, mix_here, preferred_element_type=jnp.float32).astype(jnp.bfloat16)

    def split_heads(token_level, width):
        return (
            token_level.astype(jnp.float32)
            .reshape(blocks, BLOCK, heads_here, width)
            .transpose(2, 0, 1, 3)
        )

    queries = split_heads(query_part, KEY_CHANNELS) * KEY_CHANNELS ** (-0.5)
    key_rows = split_heads(key_part, KEY_CHANNELS)
    value_rows = split_heads(value_part, DV)
    up_here = lax.dynamic_slice_in_dim(decay_outer_weight, tp_index * qk_cols, qk_cols, 2)
    bias_here = lax.dynamic_slice_in_dim(channel_decay_bias, tp_index * qk_cols, qk_cols, 1)
    spike_amounts = spike_log_decay.T[:, :, None]

    def log_decay(direction):
        preactivation = (
            jnp.dot(
                low_rank[:, direction * RANK : (direction + 1) * RANK],
                up_here[direction],
                preferred_element_type=jnp.float32,
            )
            + bias_here[direction]
        )
        token_level = (jax.nn.log_sigmoid(preactivation) / gate_norm_factor).reshape(
            sequence_length, heads_here, KEY_CHANNELS
        ) + spike_amounts
        return token_level.reshape(blocks, BLOCK, heads_here, KEY_CHANNELS).transpose(2, 0, 1, 3)

    cum_fwd = jnp.cumsum(log_decay(0), axis=2)
    cum_bwd = jnp.flip(jnp.cumsum(jnp.flip(log_decay(1), 2), axis=2), 2)
    scaled_fwd, inner_fwd = within_blocks(queries, cum_fwd, key_rows, value_rows, True)
    scaled_bwd, inner_bwd = within_blocks(queries, cum_bwd, key_rows, value_rows, False)
    edge_fwd = cum_fwd[:, :, -1, :]
    edge_bwd = cum_bwd[:, :, 0, :]
    updates_fwd = block_updates(key_rows, value_rows, cum_fwd, edge_fwd)
    updates_bwd = block_updates(key_rows, value_rows, cum_bwd, edge_bwd)
    total_fwd, before_fwd = local_chain(
        jnp.moveaxis(edge_fwd, 1, 0), jnp.moveaxis(updates_fwd, 1, 0), False
    )
    total_bwd, before_bwd = local_chain(
        jnp.moveaxis(edge_bwd, 1, 0), jnp.moveaxis(updates_bwd, 1, 0), True
    )
    neutral = (jnp.zeros_like(total_fwd[0]), jnp.zeros_like(total_fwd[1]))
    prefix_fwd = carried_in(total_fwd, SP, chain_combine, neutral)
    prefix_bwd = carried_in_2(total_bwd, SP, chain_combine, neutral)
    entering_fwd = jnp.exp(prefix_fwd[0])[..., None] * starting_state[0] + prefix_fwd[1]
    entering_bwd = jnp.exp(prefix_bwd[0])[..., None] * starting_state[1] + prefix_bwd[1]
    out_fwd = inner_fwd + carried_term(scaled_fwd, before_fwd, entering_fwd)
    out_bwd = inner_bwd + carried_term(scaled_bwd, before_bwd, entering_bwd)
    joined = out_fwd + out_bwd
    normal_scale = lax.rsqrt(jnp.mean(joined * joined, axis=-1, keepdims=True) + eps_value)
    attention_output = (
        (joined * normal_scale)
        .astype(jnp.bfloat16)
        .transpose(1, 2, 0, 3)
        .reshape(sequence_length, heads_here * DV)
    )
    whole_pool, whole_attention = gather_turned(
        (pooling_output_weight, attention_output_weight), SP, (1, 1)
    )
    part_one = jnp.dot(pool_output, whole_pool, preferred_element_type=jnp.float32)
    part_two = jnp.dot(attention_output, whole_attention, preferred_element_type=jnp.float32)
    mixed = sum_at_owner((part_one + part_two).astype(jnp.bfloat16), "tp", 0)
    return mixed.astype(jnp.bfloat16)


def solution(mesh):
    split = Mesh(mesh.devices.reshape(8, 8, 2, mesh.shape["tp"]), ("sp_0", "sp_1", "sp_2", "tp"))
    in_specs = (
        P(SP_TP, None),
        P(SP, "tp"),
        P(SP, "tp"),
        P(SP, "tp"),
        P(SP, "tp"),
        P(),
        P(),
        P(),
        P("tp", SP),
        P(None, "tp", None, None),
        P(),
        P("tp", SP),
        P("tp", SP),
    )
    out_specs = P(SP_TP, None)
    return jax.shard_map(
        shards, mesh=split, in_specs=in_specs, out_specs=out_specs, check_vma=False
    )
```

profile of v0, /device:TPU:2, one launch (start us, length us, event | category | flops | bytes accessed | tf_op | source)
XLA Modules:
  0.0 326.1 jit_solution(17219555616986555512)
XLA Ops:
  12.0 9.6 %all-to-all-start = ((bf16[4,128,2048]{2,1,0:T(8,128)(2,1)}), bf16[4,128,2048]{2,1,0:T(8,128)(2,1)S(1)}, u32[]{:S(2)}, u32[]{:S(2)}) async-start(bf16[4,128,2048]{2,1,0:T(8,128)(2,1)} %broadcast_in_dim.42), calls=%async_computation | async-start | bytes 4194304 | tf_op jit(solution)/shard_map/all_to_all | solution.py:20
  24.8 17.1 %all-to-all-done = bf16[4,128,2048]{2,1,0:T(8,128)(2,1)S(1)} async-done(((bf16[4,128,2048]{2,1,0:T(8,128)(2,1)}), bf16[4,128,2048]{2,1,0:T(8,128)(2,1)S(1)}, u32[]{:S(2)}, u32[]{:S(2)}) %all-to-all-start) | async-done | bytes 2097184 | tf_op jit(solution)/shard_map/all_to_all | solution.py:20
  46.8 1.9 rev.7
  51.6 2.1 reshape.1391
  56.3 42.6 %all-gather.12.cloned.1.call-done = bf16[2048,768]{1,0:T(8,128)(2,1)} async-done(((bf16[16,768]{1,0:T(8,128)(2,1)}), bf16[2048,768]{1,0:T(8,128)(2,1)}) %all-gather.12.cloned.1.call-update) | async-done | bytes 3145744 | tf_op jit(solution)/shard_map/all_gather | solution.py:211
  98.9 3.7 %convolution_convert_fusion = bf16[512,768]{1,0:T(8,128)(2,1)S(1)} fusion(bf16[512,2048]{1,0:T(8,128)(2,1)S(1)} %bitcast.287, bf16[2048,768]{1,0:T(8,128)(2,1)} %all-gather.12.cloned.1.call-done), kind=kOutput, calls=%fused_computation.13 | convolution fusion | flops 1611005952 | bytes 6029312 | tf_op jit(solution)/shard_map/dot_general | solution.py:209
  105.5 2.8 bitcast_multiply_fusion.1
  108.6 7.0 %while.39 = (s32[]{:T(128)}, f32[2,64]{1,0:T(2,128)S(1)}, f32[2,64,128]{2,1,0:T(8,128)S(1)}, f32[8,2,64]{2,1,0:T(2,128)S(1)}, f32[8,2,64,128]{3,2,1,0:T(8,128)S(...) while((s32[]{:T(128)}, f32[2,64]{1,0:T(2,128)S(1)}, ...), condition=%wide.region_6.7_spmd.clone, body=%wide.region_5.6_spmd.clone.sunk | while | flops 65924 | bytes 333454 | solution.py:159
  115.7 1.8 all-gather.6
  117.7 24.9 %all-gather.7 = bf16[8,129,128]{2,1,0:T(8,128)(2,1)S(1)} all-gather(bf16[1,129,128]{2,1,0:T(8,128)(2,1)S(1)} %maximum_bitcast_fusion.1), channel_id=5, replica_groups=mesh['sp_0'=8,'sp_1'=8,'sp_2'=2,'tp'=4] {'sp_1'}, dimensions={0}, use_global_device_ids=true | all-gather | bytes 297216 | tf_op jit(solution)/shard_map/all_gather | solution.py:82
  142.9 25.0 %all-gather.8 = bf16[8,129,128]{2,1,0:T(8,128)(2,1)S(1)} all-gather(bf16[1,129,128]{2,1,0:T(8,128)(2,1)S(1)} %maximum_bitcast_fusion.2), channel_id=6, replica_groups=mesh['sp_0'=8,'sp_1'=8,'sp_2'=2,'tp'=4] {'sp_0'}, dimensions={0}, use_global_device_ids=true | all-gather | bytes 297216 | tf_op jit(solution)/shard_map/all_gather | solution.py:82
  181.8 7.0 %while.38 = (s32[]{:T(128)}, f32[2,64]{1,0:T(2,128)S(1)}, f32[2,64,128]{2,1,0:T(8,128)S(1)}, f32[8,2,64]{2,1,0:T(2,128)S(1)}, f32[8,2,64,128]{3,2,1,0:T(8,128)S(...) while((s32[]{:T(128)}, f32[2,64]{1,0:T(2,128)S(1)}, ...), condition=%wide.region_3.4_spmd.clone, body=%wide.region_2.3_spmd.clone.sunk | while | flops 65923 | bytes 333434 | solution.py:159
  189.0 1.8 all-gather.5
  190.8 15.0 %all_gather.56 = bf16[8,2,64]{2,1,0:T(2,128)(2,1)S(1)} all-gather(bf16[1,2,64]{2,1,0:T(2,128)(2,1)S(1)} %get-tuple-element.410), channel_id=1, replica_groups=mesh['sp_0'=8,'sp_1'=8,'sp_2'=2,'tp'=4] {'sp_1'}, dimensions={0}, use_global_device_ids=true | all-gather | bytes 2304 | tf_op jit(solution)/shard_map/all_gather | solution.py:59
  205.9 14.8 %all_gather.57 = bf16[8,2,64]{2,1,0:T(2,128)(2,1)S(1)} all-gather(bf16[1,2,64]{2,1,0:T(2,128)(2,1)S(1)} %get-tuple-element.398), channel_id=1, replica_groups=mesh['sp_0'=8,'sp_1'=8,'sp_2'=2,'tp'=4] {'sp_0'}, dimensions={0}, use_global_device_ids=true | all-gather | bytes 2304 | tf_op jit(solution)/shard_map/all_gather | solution.py:59
  220.7 1.8 all-gather.1
  222.5 2.1 collective-permute-start
  226.0 28.0 %all_gather.60 = bf16[8,2,64,128]{3,2,1,0:T(8,128)(2,1)S(1)} all-gather(bf16[1,2,64,128]{3,2,1,0:T(8,128)(2,1)S(1)} %fusion.138), channel_id=1, replica_groups=mesh['sp_0'=8,'sp_1'=8,'sp_2'=2,'tp'=4] {'sp_1'}, dimensions={0}, use_global_device_ids=true | all-gather | bytes 294912 | tf_op jit(solution)/shard_map/all_gather | solution.py:59
  254.2 26.6 %all_gather.61 = bf16[8,2,64,128]{3,2,1,0:T(8,128)(2,1)S(1)} all-gather(bf16[1,2,64,128]{3,2,1,0:T(8,128)(2,1)S(1)} %fusion.137), channel_id=1, replica_groups=mesh['sp_0'=8,'sp_1'=8,'sp_2'=2,'tp'=4] {'sp_0'}, dimensions={0}, use_global_device_ids=true | all-gather | bytes 294912 | tf_op jit(solution)/shard_map/all_gather | solution.py:59
  281.7 1.9 fusion.126
  285.7 2.1 fusion.3
  290.3 5.1 %fusion.5 = f32[512,2048]{1,0:T(8,128)} fusion(bf16[2048,512]{1,0:T(8,128)(2,1)} %all-gather.14.cloned.1.call-done, f32[528,256]{1,0:T(8,128)S(1)} %maximum_convert_fusion, f32[512]{0:T(512)S(1)} %copy-done.15, f32[]{:T(128)S(6)} %convert_element_type.1186, f32[]{:T(128)S(6)} %convert_element_type.1185, f32[]{:T(128)S(6)} %convert_element_type.1184, ...), kind=kOutput, calls=%fused_computation.26 | convolution fusion | flops 608567296 | bytes 13764676 | tf_op jit(solution)/shard_map/dot_general | solution.py:307
  295.4 2.9 add_convert_fusion
  298.3 19.7 %all_to_all.10 = bf16[4,128,2048]{2,1,0:T(8,128)(2,1)S(1)} all-to-all(bf16[4,128,2048]{2,1,0:T(8,128)(2,1)S(1)} %bitcast.288), channel_id=1, replica_groups=mesh['sp_0'=8,'sp_1'=8,'sp_2'=2,'tp'=4] {'tp'}, dimensions={0} | all-to-all | bytes 4194304 | tf_op jit(solution)/shard_map/all_to_all | solution.py:134
  (258 shorter events, 57.8 us)
Async XLA Ops:
  6.5 283.8 %copy-start = (bf16[4,256,256]{2,1,0:T(8,128)(2,1)S(1)}, bf16[4,256,256]{2,1,0:T(8,128)(2,1)}, u32[]{:S(2)}) copy-start(bf16[4,256,256]{2,1,0:T(8,128)(2,1)} %param.27) | copy-start | bytes 1572868
  6.5 92.3 %all-gather.12.cloned.1.call-start = ((), (), s32[]{:S(2)}) async-start(), calls=%async_computation.2 | async-start | bytes 3170304 | tf_op jit(solution)/shard_map/all_gather | solution.py:211
  12.0 29.8 %all-to-all-start = ((bf16[4,128,2048]{2,1,0:T(8,128)(2,1)}), bf16[4,128,2048]{2,1,0:T(8,128)(2,1)S(1)}, u32[]{:S(2)}, u32[]{:S(2)}) async-start(bf16[4,128,2048]{2,1,0:T(8,128)(2,1)} %broadcast_in_dim.42), calls=%async_computation | async-start | bytes 4194304 | tf_op jit(solution)/shard_map/all_to_all | solution.py:20
  21.6 268.7 %all-gather.14.cloned.1.call-start = ((), (), s32[]{:S(2)}) async-start(), calls=%async_computation.3 | async-start | bytes 2113536 | tf_op jit(solution)/shard_map/all_gather | solution.py:118
  188.8 94.9 %copy-start.8 = (f32[2,2,64,128]{3,2,1,0:T(8,128)S(1)}, f32[2,2,64,128]{3,2,1,0:T(8,128)}, u32[]{:S(2)}) copy-start(f32[2,2,64,128]{3,2,1,0:T(8,128)} %param.26) | copy-start | bytes 393220
  188.8 94.9 %copy-start.16 = (f32[2,64]{1,0:T(2,128)S(1)}, f32[2,64]{1,0:T(2,128)}, u32[]{:S(2)}) copy-start(f32[2,64]{1,0:T(2,128)} %reshape.1519) | copy-start | bytes 1540
  188.8 94.9 %copy-start.17 = (f32[2,64]{1,0:T(2,128)S(1)}, f32[2,64]{1,0:T(2,128)}, u32[]{:S(2)}) copy-start(f32[2,64]{1,0:T(2,128)} %reshape.1557) | copy-start | bytes 1540
  188.8 94.9 %copy-start.18 = (f32[2,64]{1,0:T(2,128)S(1)}, f32[2,64]{1,0:T(2,128)}, u32[]{:S(2)}) copy-start(f32[2,64]{1,0:T(2,128)} %reshape.1568) | copy-start | bytes 1540
  188.8 94.9 %copy-start.19 = (f32[2,64]{1,0:T(2,128)S(1)}, f32[2,64]{1,0:T(2,128)}, u32[]{:S(2)}) copy-start(f32[2,64]{1,0:T(2,128)} %exp.501) | copy-start | bytes 1540
  188.8 94.9 %copy-start.20 = (f32[2,64]{1,0:T(2,128)S(1)}, f32[2,64]{1,0:T(2,128)}, u32[]{:S(2)}) copy-start(f32[2,64]{1,0:T(2,128)} %exp.503) | copy-start | bytes 1540
  188.9 94.9 %copy-start.21 = (f32[2,64]{1,0:T(2,128)S(1)}, f32[2,64]{1,0:T(2,128)}, u32[]{:S(2)}) copy-start(f32[2,64]{1,0:T(2,128)} %exp.505) | copy-start | bytes 1540
  188.9 94.9 %copy-start.22 = (f32[2,64]{1,0:T(2,128)S(1)}, f32[2,64]{1,0:T(2,128)}, u32[]{:S(2)}) copy-start(f32[2,64]{1,0:T(2,128)} %mul.911) | copy-start | bytes 1540
  188.9 94.9 %copy-start.23 = (f32[2,64]{1,0:T(2,128)S(1)}, f32[2,64]{1,0:T(2,128)}, u32[]{:S(2)}) copy-start(f32[2,64]{1,0:T(2,128)} %reshape.1462) | copy-start | bytes 1540
  188.9 94.9 %copy-start.24 = (f32[2,64]{1,0:T(2,128)S(1)}, f32[2,64]{1,0:T(2,128)}, u32[]{:S(2)}) copy-start(f32[2,64]{1,0:T(2,128)} %reshape.1480) | copy-start | bytes 1540
  188.9 94.9 %copy-start.25 = (f32[2,64]{1,0:T(2,128)S(1)}, f32[2,64]{1,0:T(2,128)}, u32[]{:S(2)}) copy-start(f32[2,64]{1,0:T(2,128)} %reshape.1497) | copy-start | bytes 1540
  188.9 94.9 %copy-start.26 = (f32[2,64]{1,0:T(2,128)S(1)}, f32[2,64]{1,0:T(2,128)}, u32[]{:S(2)}) copy-start(f32[2,64]{1,0:T(2,128)} %exp.512) | copy-start | bytes 1540
  188.9 94.9 %copy-start.27 = (f32[2,64]{1,0:T(2,128)S(1)}, f32[2,64]{1,0:T(2,128)}, u32[]{:S(2)}) copy-start(f32[2,64]{1,0:T(2,128)} %exp.513) | copy-start | bytes 1540
  188.9 94.9 %copy-start.28 = (f32[2,64]{1,0:T(2,128)S(1)}, f32[2,64]{1,0:T(2,128)}, u32[]{:S(2)}) copy-start(f32[2,64]{1,0:T(2,128)} %exp.514) | copy-start | bytes 1540
  188.9 94.9 %copy-start.29 = (f32[2,64]{1,0:T(2,128)S(1)}, f32[2,64]{1,0:T(2,128)}, u32[]{:S(2)}) copy-start(f32[2,64]{1,0:T(2,128)} %mul.929) | copy-start | bytes 1540
  188.9 94.9 %copy-start.30 = (f32[2,64]{1,0:T(2,128)S(1)}, f32[2,64]{1,0:T(2,128)}, u32[]{:S(2)}) copy-start(f32[2,64]{1,0:T(2,128)} %reshape.1463) | copy-start | bytes 1540
  189.0 94.9 %copy-start.31 = (f32[2,64]{1,0:T(2,128)S(1)}, f32[2,64]{1,0:T(2,128)}, u32[]{:S(2)}) copy-start(f32[2,64]{1,0:T(2,128)} %reshape.1481) | copy-start | bytes 1540
  189.0 94.9 %copy-start.32 = (f32[2,64]{1,0:T(2,128)S(1)}, f32[2,64]{1,0:T(2,128)}, u32[]{:S(2)}) copy-start(f32[2,64]{1,0:T(2,128)} %reshape.1498) | copy-start | bytes 1540
  222.5 67.7 %collective-permute-start = (bf16[8,256]{1,0:T(8,128)(2,1)}, bf16[8,256]{1,0:T(8,128)(2,1)S(1)}, u32[]{:S(2)}, u32[]{:S(2)}) collective-permute-start(bf16[8,256]{1,0:T(8,128)(2,1)} %get-tuple-element.350), channel_id=1, source_target_pairs={{0,4},{4,8},{8,12},{12,16},{16,20},{20,24},{24,28},{28,32},{32,36}... | collective-permute-start | bytes 12296 | tf_op jit(solution)/shard_map/ppermute | solution.py:41
  224.6 65.6 %collective-permute-start.1 = (bf16[8,256]{1,0:T(8,128)(2,1)}, bf16[8,256]{1,0:T(8,128)(2,1)S(1)}, u32[]{:S(2)}, u32[]{:S(2)}) collective-permute-start(bf16[8,256]{1,0:T(8,128)(2,1)} %get-tuple-element.351), channel_id=1, source_target_pairs={{4,0},{8,4},{12,8},{16,12},{20,16},{24,20},{28,24},{32,28},{36,32}... | collective-permute-start | bytes 12296 | tf_op jit(solution)/shard_map/ppermute | solution.py:42
  (18 other events, 554.5 us)
Sparse Core Ops, SparseCore 0:
  10.5 88.3 all-gather.11
  102.0 80.1 all-gather.13
where the time goes:
time: 328 us; the launch traced here: 326 us
  blocking collectives  159 us (48%)
  waiting for transfers between devices  59.8 us (18%)
  local copies, waits for them, and re-layouts  37.4 us (11%)
  matrix products  21.7 us (7%)
  other arithmetic  19.6 us (6%)
  between operations  14.6 us (4%)
  starting transfers between devices  13 us (4%)
    all_gather x6, blocking collectives, carried_in(): lax.all_gather(part.astype(kind), axis)  88 us
    all_gather x3, blocking collectives, gathered_once(): both, at, found = (lax.all_gather(jnp.concatenate(lines), axis), 0, {})  51.7 us
    all_gather x1, waiting for transfers between devices, shards(): lax.all_gather(local_weight, SP, axis=0, tiled=True)  42.6 us
    all_to_all x1, blocking collectives, sum_at_owner(): lax.all_to_all(cut_along(value, dim, devices), axis, 0, 0, tiled=True)  19.7 us
    all_to_all x1, waiting for transfers between devices, from_everyone(): return lax.all_to_all(copies, axis, split_axis=0, concat_axis=0, tiled=True)  17.1 us
    dynamic_slice x16, local copies, waits for them, and re-layouts, local_chain(): return lax.scan(advance, begin, (decays, updates), reverse=backward)  11.3 us
    exp x19, local copies, waits for them, and re-layouts, chain_combine(): jnp.exp(later[0])[..., None] * earlier[1] + later[1]  11 us
    all_to_all x1, starting transfers between devices, from_everyone(): return lax.all_to_all(copies, axis, split_axis=0, concat_axis=0, tiled=True)  9.6 us
  transfers between devices with their start and end apart: 5, of which 2 were waited for; matrix products, arithmetic and copies ran while one was open for 21% of the time, Pallas kernels for 0%

commit v1 on v0

--- a/solution.py
+++ b/solution.py
@@ -13,6 +13,11 @@
 eps_value = 1e-06
 gate_norm_factor = 16.0
 rim_width = 8
+
+
+def exchange_gather(value, name, dim):
+    repeated = jnp.stack([value] * lax.axis_size(name))
+    return jnp.concatenate(lax.all_to_all(repeated, name, 0, 0), axis=dim)
 
 
 def from_everyone(value, axis):
@@ -207,9 +212,7 @@
     )
     all_rows = gathered_copies(normed, "tp", 0)
     summed = jnp.dot(
-        all_rows,
-        lax.all_gather(local_weight, SP, axis=0, tiled=True),
-        preferred_element_type=jnp.float32,
+        all_rows, exchange_gather(local_weight, SP, 0), preferred_element_type=jnp.float32
     )
     rank_part = jnp.dot(all_rows, decay_inner_weight, preferred_element_type=jnp.float32).astype(
         jnp.bfloat16

time: 328 us -> 363 us (1.11)
  waiting for transfers between devices: 59.8 us -> 78.2 us
  starting transfers between devices: 13 us -> 31.4 us
    all_to_all x0 -> x1, waiting for transfers between devices: none -> 57.9 us  [exchange_gather(): return jnp.concatenate(lax.all_to_all(repeated, name, 0, 0), axis=dim)]
    all_gather x1 -> x0, waiting for transfers between devices: 42.6 us -> none  [shards(): lax.all_gather(local_weight, SP, axis=0, tiled=True)]
    all_to_all x0 -> x1, starting transfers between devices: none -> 18.4 us  [exchange_gather(): return jnp.concatenate(lax.all_to_all(repeated, name, 0, 0), axis=dim)]
  transfers between devices with their start and end apart: 5 -> 5, of which waited for: 2 -> 2; matrix products, arithmetic and copies ran while one was open for 21% -> 17% of each run, Pallas kernels for 0% -> 0%
where the time goes in v1:
time: 363 us; the launch traced here: 361 us
  blocking collectives  159 us (44%)
  waiting for transfers between devices  78.2 us (22%)
  local copies, waits for them, and re-layouts  38.4 us (11%)
  starting transfers between devices  31.4 us (9%)
  matrix products  20.9 us (6%)
  other arithmetic  18.3 us (5%)
  between operations  14.7 us (4%)
    all_gather x6, blocking collectives, carried_in(): lax.all_gather(part.astype(kind), axis)  87.6 us
    all_to_all x1, waiting for transfers between devices, exchange_gather(): return jnp.concatenate(lax.all_to_all(repeated, name, 0, 0), axis=dim)  57.9 us
    all_gather x3, blocking collectives, gathered_once(): both, at, found = (lax.all_gather(jnp.concatenate(lines), axis), 0, {})  52.3 us
    all_to_all x1, waiting for transfers between devices, from_everyone(): return lax.all_to_all(copies, axis, split_axis=0, concat_axis=0, tiled=True)  20.2 us
    all_to_all x1, blocking collectives, sum_at_owner(): lax.all_to_all(cut_along(value, dim, devices), axis, 0, 0, tiled=True)  19.1 us
    all_to_all x1, starting transfers between devices, exchange_gather(): return jnp.concatenate(lax.all_to_all(repeated, name, 0, 0), axis=dim)  18.4 us
    dynamic_slice x16, local copies, waits for them, and re-layouts, local_chain(): return lax.scan(advance, begin, (decays, updates), reverse=backward)  11.3 us
    exp x19, local copies, waits for them, and re-layouts, chain_combine(): jnp.exp(later[0])[..., None] * earlier[1] + later[1]  10.9 us
  transfers between devices with their start and end apart: 5, of which 2 were waited for; matrix products, arithmetic and copies ran while one was open for 17% of the time, Pallas kernels for 0%

profile of v1, /device:TPU:2, one launch (start us, length us, event | category | flops | bytes accessed | tf_op | source)
XLA Modules:
  0.0 361.4 jit_solution(13412414644414750431)
XLA Ops:
  10.7 9.6 %all-to-all-start = ((bf16[4,128,2048]{2,1,0:T(8,128)(2,1)}), bf16[4,128,2048]{2,1,0:T(8,128)(2,1)S(1)}, u32[]{:S(2)}, u32[]{:S(2)}) async-start(bf16[4,128,2048]{2,1,0:T(8,128)(2,1)} %broadcast_in_dim.42), calls=%async_computation | async-start | bytes 4194304 | tf_op jit(solution)/shard_map/all_to_all | solution.py:25
  20.3 20.2 %all-to-all-done = bf16[4,128,2048]{2,1,0:T(8,128)(2,1)S(1)} async-done(((bf16[4,128,2048]{2,1,0:T(8,128)(2,1)}), bf16[4,128,2048]{2,1,0:T(8,128)(2,1)S(1)}, u32[]{:S(2)}, u32[]{:S(2)}) %all-to-all-start) | async-done | bytes 2097184 | tf_op jit(solution)/shard_map/all_to_all | solution.py:25
  40.5 1.9 stack.2
  42.4 18.4 %all-to-all-start.1 = ((bf16[128,16,768]{2,1,0:T(8,128)(2,1)}), bf16[128,16,768]{2,1,0:T(8,128)(2,1)}, u32[]{:S(2)}, u32[]{:S(2)}) async-start(bf16[128,16,768]{2,1,0:T(8,128)(2,1)} %stack.2), calls=%async_computation.1 | async-start | bytes 6291456 | tf_op jit(solution)/shard_map/all_to_all | solution.py:20
  68.9 1.9 rev.7
  76.8 57.9 %all-to-all-done.1 = bf16[128,16,768]{2,1,0:T(8,128)(2,1)} async-done(((bf16[128,16,768]{2,1,0:T(8,128)(2,1)}), bf16[128,16,768]{2,1,0:T(8,128)(2,1)}, u32[]{:S(2)}, u32[]{:S(2)}) %all-to-all-start.1) | async-done | bytes 3145760 | tf_op jit(solution)/shard_map/all_to_all | solution.py:20
  134.7 3.7 %convolution_convert_fusion = bf16[512,768]{1,0:T(8,128)(2,1)S(1)} fusion(bf16[512,2048]{1,0:T(8,128)(2,1)S(1)} %bitcast.288, bf16[2048,768]{1,0:T(8,128)(2,1)} %bitcast.1), kind=kOutput, calls=%fused_computation.13 | convolution fusion | flops 1611005952 | bytes 6029312 | tf_op jit(solution)/shard_map/dot_general | solution.py:214
  141.4 2.8 bitcast_multiply_fusion.1
  144.5 7.0 %while.39 = (s32[]{:T(128)}, f32[2,64]{1,0:T(2,128)S(1)}, f32[2,64,128]{2,1,0:T(8,128)S(1)}, f32[8,2,64]{2,1,0:T(2,128)S(1)}, f32[8,2,64,128]{3,2,1,0:T(8,128)S(...) while((s32[]{:T(128)}, f32[2,64]{1,0:T(2,128)S(1)}, ...), condition=%wide.region_6.7_spmd.clone, body=%wide.region_5.6_spmd.clone.sunk | while | flops 65924 | bytes 333454 | solution.py:164
  151.6 1.8 all-gather.6
  153.6 25.6 %all-gather.7 = bf16[8,129,128]{2,1,0:T(8,128)(2,1)S(1)} all-gather(bf16[1,129,128]{2,1,0:T(8,128)(2,1)S(1)} %maximum_bitcast_fusion.1), channel_id=5, replica_groups=mesh['sp_0'=8,'sp_1'=8,'sp_2'=2,'tp'=4] {'sp_1'}, dimensions={0}, use_global_device_ids=true | all-gather | bytes 297216 | tf_op jit(solution)/shard_map/all_gather | solution.py:87
  179.4 24.9 %all-gather.8 = bf16[8,129,128]{2,1,0:T(8,128)(2,1)S(1)} all-gather(bf16[1,129,128]{2,1,0:T(8,128)(2,1)S(1)} %maximum_bitcast_fusion.2), channel_id=6, replica_groups=mesh['sp_0'=8,'sp_1'=8,'sp_2'=2,'tp'=4] {'sp_0'}, dimensions={0}, use_global_device_ids=true | all-gather | bytes 297216 | tf_op jit(solution)/shard_map/all_gather | solution.py:87
  218.2 7.0 %while.38 = (s32[]{:T(128)}, f32[2,64]{1,0:T(2,128)S(1)}, f32[2,64,128]{2,1,0:T(8,128)S(1)}, f32[8,2,64]{2,1,0:T(2,128)S(1)}, f32[8,2,64,128]{3,2,1,0:T(8,128)S(...) while((s32[]{:T(128)}, f32[2,64]{1,0:T(2,128)S(1)}, ...), condition=%wide.region_3.4_spmd.clone, body=%wide.region_2.3_spmd.clone.sunk | while | flops 65923 | bytes 333434 | solution.py:164
  227.2 16.5 %all_gather.52 = bf16[8,2,64]{2,1,0:T(2,128)(2,1)S(1)} all-gather(bf16[1,2,64]{2,1,0:T(2,128)(2,1)S(1)} %get-tuple-element.410), channel_id=1, replica_groups=mesh['sp_0'=8,'sp_1'=8,'sp_2'=2,'tp'=4] {'sp_1'}, dimensions={0}, use_global_device_ids=true | all-gather | bytes 2304 | tf_op jit(solution)/shard_map/all_gather | solution.py:64
  243.8 14.7 %all_gather.53 = bf16[8,2,64]{2,1,0:T(2,128)(2,1)S(1)} all-gather(bf16[1,2,64]{2,1,0:T(2,128)(2,1)S(1)} %get-tuple-element.398), channel_id=1, replica_groups=mesh['sp_0'=8,'sp_1'=8,'sp_2'=2,'tp'=4] {'sp_0'}, dimensions={0}, use_global_device_ids=true | all-gather | bytes 2304 | tf_op jit(solution)/shard_map/all_gather | solution.py:64
  258.5 1.8 all-gather.1
  260.3 2.1 collective-permute-start
  263.8 26.5 %all_gather.56 = bf16[8,2,64,128]{3,2,1,0:T(8,128)(2,1)S(1)} all-gather(bf16[1,2,64,128]{3,2,1,0:T(8,128)(2,1)S(1)} %fusion.138), channel_id=1, replica_groups=mesh['sp_0'=8,'sp_1'=8,'sp_2'=2,'tp'=4] {'sp_1'}, dimensions={0}, use_global_device_ids=true | all-gather | bytes 294912 | tf_op jit(solution)/shard_map/all_gather | solution.py:64
  290.5 26.2 %all_gather.57 = bf16[8,2,64,128]{3,2,1,0:T(8,128)(2,1)S(1)} all-gather(bf16[1,2,64,128]{3,2,1,0:T(8,128)(2,1)S(1)} %fusion.137), channel_id=1, replica_groups=mesh['sp_0'=8,'sp_1'=8,'sp_2'=2,'tp'=4] {'sp_0'}, dimensions={0}, use_global_device_ids=true | all-gather | bytes 294912 | tf_op jit(solution)/shard_map/all_gather | solution.py:64
  317.6 1.9 fusion.126
  321.6 2.1 fusion.3
  326.2 4.9 %fusion.5 = f32[512,2048]{1,0:T(8,128)} fusion(bf16[2048,512]{1,0:T(8,128)(2,1)} %all-gather.11.cloned.1.call-done, f32[528,256]{1,0:T(8,128)S(1)} %maximum_convert_fusion, f32[512]{0:T(512)S(1)} %copy-done.19, f32[]{:T(128)S(6)} %convert_element_type.1186, f32[]{:T(128)S(6)} %convert_element_type.1185, f32[]{:T(128)S(6)} %convert_element_type.1184, ...), kind=kOutput, calls=%fused_computation.26 | convolution fusion | flops 608567296 | bytes 13764676 | tf_op jit(solution)/shard_map/dot_general | solution.py:310
  331.2 2.9 add_convert_fusion
  334.1 19.1 %all_to_all.15 = bf16[4,128,2048]{2,1,0:T(8,128)(2,1)S(1)} all-to-all(bf16[4,128,2048]{2,1,0:T(8,128)(2,1)S(1)} %bitcast.289), channel_id=1, replica_groups=mesh['sp_0'=8,'sp_1'=8,'sp_2'=2,'tp'=4] {'tp'}, dimensions={0} | all-to-all | bytes 4194304 | tf_op jit(solution)/shard_map/all_to_all | solution.py:139
  (266 shorter events, 58.5 us)
Async XLA Ops:
  6.5 319.7 %copy-start = (bf16[4,256,256]{2,1,0:T(8,128)(2,1)S(1)}, bf16[4,256,256]{2,1,0:T(8,128)(2,1)}, u32[]{:S(2)}) copy-start(bf16[4,256,256]{2,1,0:T(8,128)(2,1)} %param.27) | copy-start | bytes 1572868
  10.7 29.8 %all-to-all-start = ((bf16[4,128,2048]{2,1,0:T(8,128)(2,1)}), bf16[4,128,2048]{2,1,0:T(8,128)(2,1)S(1)}, u32[]{:S(2)}, u32[]{:S(2)}) async-start(bf16[4,128,2048]{2,1,0:T(8,128)(2,1)} %broadcast_in_dim.42), calls=%async_computation | async-start | bytes 4194304 | tf_op jit(solution)/shard_map/all_to_all | solution.py:25
  42.4 92.3 %all-to-all-start.1 = ((bf16[128,16,768]{2,1,0:T(8,128)(2,1)}), bf16[128,16,768]{2,1,0:T(8,128)(2,1)}, u32[]{:S(2)}, u32[]{:S(2)}) async-start(bf16[128,16,768]{2,1,0:T(8,128)(2,1)} %stack.2), calls=%async_computation.1 | async-start | bytes 6291456 | tf_op jit(solution)/shard_map/all_to_all | solution.py:20
  60.8 265.4 %all-gather.11.cloned.1.call-start = ((), (), s32[]{:S(2)}) async-start(), calls=%async_computation.3 | async-start | bytes 2113536 | tf_op jit(solution)/shard_map/all_gather | solution.py:123
  225.1 94.4 %copy-start.8 = (f32[2,2,64,128]{3,2,1,0:T(8,128)S(1)}, f32[2,2,64,128]{3,2,1,0:T(8,128)}, u32[]{:S(2)}) copy-start(f32[2,2,64,128]{3,2,1,0:T(8,128)} %param.26) | copy-start | bytes 393220
  225.2 94.4 %copy-start.20 = (f32[2,64]{1,0:T(2,128)S(1)}, f32[2,64]{1,0:T(2,128)}, u32[]{:S(2)}) copy-start(f32[2,64]{1,0:T(2,128)} %reshape.1525) | copy-start | bytes 1540
  225.2 94.4 %copy-start.21 = (f32[2,64]{1,0:T(2,128)S(1)}, f32[2,64]{1,0:T(2,128)}, u32[]{:S(2)}) copy-start(f32[2,64]{1,0:T(2,128)} %reshape.1563) | copy-start | bytes 1540
  225.2 94.4 %copy-start.22 = (f32[2,64]{1,0:T(2,128)S(1)}, f32[2,64]{1,0:T(2,128)}, u32[]{:S(2)}) copy-start(f32[2,64]{1,0:T(2,128)} %reshape.1574) | copy-start | bytes 1540
  225.2 94.4 %copy-start.23 = (f32[2,64]{1,0:T(2,128)S(1)}, f32[2,64]{1,0:T(2,128)}, u32[]{:S(2)}) copy-start(f32[2,64]{1,0:T(2,128)} %exp.501) | copy-start | bytes 1540
  225.2 94.4 %copy-start.24 = (f32[2,64]{1,0:T(2,128)S(1)}, f32[2,64]{1,0:T(2,128)}, u32[]{:S(2)}) copy-start(f32[2,64]{1,0:T(2,128)} %exp.503) | copy-start | bytes 1540
  225.2 94.4 %copy-start.25 = (f32[2,64]{1,0:T(2,128)S(1)}, f32[2,64]{1,0:T(2,128)}, u32[]{:S(2)}) copy-start(f32[2,64]{1,0:T(2,128)} %exp.505) | copy-start | bytes 1540
  225.2 94.4 %copy-start.26 = (f32[2,64]{1,0:T(2,128)S(1)}, f32[2,64]{1,0:T(2,128)}, u32[]{:S(2)}) copy-start(f32[2,64]{1,0:T(2,128)} %mul.911) | copy-start | bytes 1540
  225.2 94.4 %copy-start.27 = (f32[2,64]{1,0:T(2,128)S(1)}, f32[2,64]{1,0:T(2,128)}, u32[]{:S(2)}) copy-start(f32[2,64]{1,0:T(2,128)} %reshape.1468) | copy-start | bytes 1540
  225.2 94.4 %copy-start.28 = (f32[2,64]{1,0:T(2,128)S(1)}, f32[2,64]{1,0:T(2,128)}, u32[]{:S(2)}) copy-start(f32[2,64]{1,0:T(2,128)} %reshape.1486) | copy-start | bytes 1540
  225.2 94.4 %copy-start.29 = (f32[2,64]{1,0:T(2,128)S(1)}, f32[2,64]{1,0:T(2,128)}, u32[]{:S(2)}) copy-start(f32[2,64]{1,0:T(2,128)} %reshape.1503) | copy-start | bytes 1540
  225.3 94.4 %copy-start.30 = (f32[2,64]{1,0:T(2,128)S(1)}, f32[2,64]{1,0:T(2,128)}, u32[]{:S(2)}) copy-start(f32[2,64]{1,0:T(2,128)} %exp.512) | copy-start | bytes 1540
  225.3 94.4 %copy-start.31 = (f32[2,64]{1,0:T(2,128)S(1)}, f32[2,64]{1,0:T(2,128)}, u32[]{:S(2)}) copy-start(f32[2,64]{1,0:T(2,128)} %exp.513) | copy-start | bytes 1540
  225.3 94.4 %copy-start.32 = (f32[2,64]{1,0:T(2,128)S(1)}, f32[2,64]{1,0:T(2,128)}, u32[]{:S(2)}) copy-start(f32[2,64]{1,0:T(2,128)} %exp.514) | copy-start | bytes 1540
  225.3 94.4 %copy-start.33 = (f32[2,64]{1,0:T(2,128)S(1)}, f32[2,64]{1,0:T(2,128)}, u32[]{:S(2)}) copy-start(f32[2,64]{1,0:T(2,128)} %mul.929) | copy-start | bytes 1540
  225.3 94.4 %copy-start.34 = (f32[2,64]{1,0:T(2,128)S(1)}, f32[2,64]{1,0:T(2,128)}, u32[]{:S(2)}) copy-start(f32[2,64]{1,0:T(2,128)} %reshape.1469) | copy-start | bytes 1540
  225.3 94.4 %copy-start.35 = (f32[2,64]{1,0:T(2,128)S(1)}, f32[2,64]{1,0:T(2,128)}, u32[]{:S(2)}) copy-start(f32[2,64]{1,0:T(2,128)} %reshape.1487) | copy-start | bytes 1540
  225.3 94.4 %copy-start.36 = (f32[2,64]{1,0:T(2,128)S(1)}, f32[2,64]{1,0:T(2,128)}, u32[]{:S(2)}) copy-start(f32[2,64]{1,0:T(2,128)} %reshape.1504) | copy-start | bytes 1540
  260.3 65.8 %collective-permute-start = (bf16[8,256]{1,0:T(8,128)(2,1)}, bf16[8,256]{1,0:T(8,128)(2,1)S(1)}, u32[]{:S(2)}, u32[]{:S(2)}) collective-permute-start(bf16[8,256]{1,0:T(8,128)(2,1)} %get-tuple-element.350), channel_id=1, source_target_pairs={{0,4},{4,8},{8,12},{12,16},{16,20},{20,24},{24,28},{28,32},{32,36}... | collective-permute-start | bytes 12296 | tf_op jit(solution)/shard_map/ppermute | solution.py:46
  262.4 63.7 %collective-permute-start.1 = (bf16[8,256]{1,0:T(8,128)(2,1)}, bf16[8,256]{1,0:T(8,128)(2,1)S(1)}, u32[]{:S(2)}, u32[]{:S(2)}) collective-permute-start(bf16[8,256]{1,0:T(8,128)(2,1)} %get-tuple-element.351), channel_id=1, source_target_pairs={{4,0},{8,4},{12,8},{16,12},{20,16},{24,20},{28,24},{32,28},{36,32}... | collective-permute-start | bytes 12296 | tf_op jit(solution)/shard_map/ppermute | solution.py:47
  (22 other events, 609.5 us)
Sparse Core Ops, SparseCore 0:
  64.8 124.9 all-gather.10
